TPU v7x, 32 devices: a whole 2x2x4 slice. The times are simulated.
32 devices in a mesh: tp: 8 (over z, x), dp: 4 (over y, core).
Axes of the slice: x: 2, y: 2, z: 4, core: 2. Of those that a mesh axis runs over, the one named last changes fastest.
Arguments:
- tokens: bfloat16 [64, 4096], P(None, 'dp'), may hold values from -6 to 6
- recurrent_state: float32 [2, 64, 262144], P(None, 'dp', 'tp'), may hold values from -24 to 24
- pre_gain: float32 [2, 4096], P(None, 'dp'), may hold values from 0.1 to 1.9
- w_query: bfloat16 [2, 4096, 2048], P(None, 'dp', 'tp'), may hold values from -0.09375 to 0.09375
- w_key: bfloat16 [2, 4096, 2048], P(None, 'dp', 'tp'), may hold values from -0.09375 to 0.09375
- w_value: bfloat16 [2, 4096, 4096], P(None, 'dp', 'tp'), may hold values from -0.09375 to 0.09375
- w_gate: bfloat16 [2, 4096, 4096], P(None, 'dp', 'tp'), may hold values from -0.09375 to 0.09375
- w_decay: bfloat16 [2, 4096, 2048], P(None, 'dp', 'tp'), may hold values from -1 to 1
- decay_bias: float32 [2, 2048], P(None, 'tp'), may hold values from -5 to 3
- head_gain: float32 [2, 128], replicated, may hold values from 0.1 to 1.9
- w_out: bfloat16 [2, 4096, 4096], P(None, 'tp', 'dp'), may hold values from -0.09375 to 0.09375
- post_gain: float32 [2, 4096], P(None, 'dp'), may hold values from 0.1 to 1.9
Outputs:
- hidden_out: bfloat16 [64, 4096], P(None, 'dp')
- state_out: float32 [2, 64, 262144], P(None, 'dp', 'tp')
All inputs are finite; a program needn't handle non-finite values.
Results may differ from a plain program's by a relative error of at most 0.015.
Values may be sent and summed in bfloat16 or wider, within the bound.
A program may use at most 64 MiB of HBM per device.

v0:
```python
import jax
import jax.numpy as jnp
from jax import lax
from jax.sharding import PartitionSpec as P

D = 4096
KEY = 64
VAL = 128
epsilon = 1e-06


def local(
    tokens,
    recurrent_state,
    pre_gain,
    w_query,
    w_key,
    w_value,
    w_gate,
    w_decay,
    decay_bias,
    head_gain,
    w_out,
    post_gain,
):
    local_seqs = recurrent_state.shape[1]
    value_cols = recurrent_state.shape[2] // KEY
    heads_here = value_cols // VAL
    highest = lax.Precision.HIGHEST
    spread = (
        jnp.arange(value_cols, dtype=jnp.int32)[None, :] // VAL
        == jnp.arange(heads_here, dtype=jnp.int32)[:, None]
    ).astype(jnp.float32)

    def spread_heads(vectors):
        shaped = vectors.astype(jnp.float32).reshape(local_seqs, heads_here, KEY)
        return jnp.einsum("bhk,hc->bck", shaped, spread, precision=highest)

    residual = tokens
    new_states = []
    for section_index in range(2):
        wide_float = residual.astype(jnp.float32)
        squares_part = jnp.sum(wide_float * wide_float, axis=1)
        normed = (wide_float * pre_gain[section_index]).astype(jnp.bfloat16)
        partials = tuple(
            (
                jnp.dot(normed, weights[section_index], preferred_element_type=jnp.float32)
                for weights in (w_query, w_key, w_value, w_gate, w_decay)
            )
        )
        summed = lax.psum_scatter(partials + (squares_part,), "dp", scatter_dimension=0, tiled=True)
        projected = summed[:5]
        own_squares = summed[5]
        row_scale = lax.rsqrt(own_squares / D + epsilon)[:, None]
        query_part = (projected[0] * row_scale).astype(jnp.bfloat16)
        key_part = (projected[1] * row_scale).astype(jnp.bfloat16)
        values_own = projected[2] * row_scale
        gate_pre = projected[3] * row_scale
        log_decay = jax.nn.log_sigmoid(projected[4] * row_scale + decay_bias[section_index]) / 16.0
        query_cols = spread_heads(query_part)
        key_cols = spread_heads(key_part)
        decay_cols = jnp.exp(spread_heads(log_decay))
        old_state = recurrent_state[section_index].reshape(local_seqs, value_cols, KEY)
        new_state = decay_cols * old_state + key_cols * values_own[:, :, None]
        readout = jnp.sum(query_cols * new_state, axis=2) * KEY ** (-0.5)
        head_mean = jnp.mean(
            (readout * readout).reshape(local_seqs, heads_here, VAL), axis=2, keepdims=True
        )
        scaled = (
            readout.reshape(local_seqs, heads_here, VAL)
            * lax.rsqrt(head_mean + epsilon)
            * head_gain[section_index]
        )
        mixed = (scaled.reshape(local_seqs, value_cols) * jax.nn.silu(gate_pre)).astype(
            jnp.bfloat16
        )
        out_weight = w_out[section_index]
        partial_out = jnp.dot(
            lax.all_gather(mixed, "dp", axis=0, tiled=True),
            out_weight,
            preferred_element_type=jnp.float32,
        )
        out_rows = lax.psum(partial_out, "tp")
        out_squares = lax.psum(jnp.sum(out_rows * out_rows, axis=1), "dp")
        residual = (
            wide_float
            + out_rows * lax.rsqrt(out_squares / D + epsilon)[:, None] * post_gain[section_index]
        ).astype(jnp.bfloat16)
        new_states.append(new_state.reshape(local_seqs, value_cols * KEY))
    return (residual, jnp.stack(new_states))


def solution(mesh):
    in_specs = (
        P(None, "dp"),
        P(None, "dp", "tp"),
        P(None, "dp"),
        P(None, "dp", "tp"),
        P(None, "dp", "tp"),
        P(None, "dp", "tp"),
        P(None, "dp", "tp"),
        P(None, "dp", "tp"),
        P(None, "tp"),
        P(),
        P(None, "tp", "dp"),
        P(None, "dp"),
    )
    out_specs = (P(None, "dp"), P(None, "dp", "tp"))
    return jax.shard_map(local, mesh=mesh, in_specs=in_specs, out_specs=out_specs, check_vma=False)
```

profile of v0, /device:TPU:0, one launch (start us, length us, event | category | flops | bytes accessed | tf_op | source)
XLA Modules:
  0.0 412.4 jit_solution(11796743993679151280)
XLA Ops:
  17.6 3.9 fusion.83
  24.5 3.8 copy.18
  28.3 8.4 %all-reduce = f32[64]{0:T(128)S(1)} all-reduce(f32[64]{0:T(128)S(1)} %fusion.41), channel_id=3, replica_groups=mesh['tp'=8,'dp'=4] {'dp'}, use_global_device_ids=true, to_apply=%region_2.3.clone | all-reduce | flops 64 | bytes 512
  38.1 16.7 %reduce-scatter.13.cloned.1.call-done = f32[16,256]{1,0:T(8,128)} async-done(((f32[64,256]{1,0:T(8,128)}), f32[16,256]{1,0:T(8,128)}) %reduce-scatter.13.cloned.1.call-update) | async-done | bytes 16400 | tf_op jit(solution)/shard_map/reduce_scatter | solution.py:51
  54.7 22.0 %reduce-scatter.15.cloned.1.call-done = f32[16,256]{1,0:T(8,128)} async-done(((f32[64,256]{1,0:T(8,128)}), f32[16,256]{1,0:T(8,128)}) %reduce-scatter.15.cloned.1.call-update) | async-done | bytes 16400 | tf_op jit(solution)/shard_map/reduce_scatter | solution.py:51
  80.2 19.1 %reduce-scatter.17.cloned.1.call-done = f32[16,512]{1,0:T(8,128)} async-done(((f32[64,512]{1,0:T(8,128)}), f32[16,512]{1,0:T(8,128)}) %reduce-scatter.17.cloned.1.call-update) | async-done | bytes 32784 | tf_op jit(solution)/shard_map/reduce_scatter | solution.py:51
  103.5 17.7 %reduce-scatter.19.cloned.1.call-done = f32[16,512]{1,0:T(8,128)} async-done(((f32[64,512]{1,0:T(8,128)}), f32[16,512]{1,0:T(8,128)}) %reduce-scatter.19.cloned.1.call-update) | async-done | bytes 32784 | tf_op jit(solution)/shard_map/reduce_scatter | solution.py:51
  122.2 5.2 %all_gather.6 = bf16[64,512]{1,0:T(8,128)(2,1)S(1)} all-gather(bf16[16,512]{1,0:T(8,128)(2,1)S(1)} %fusion.61), channel_id=1, replica_groups=mesh['tp'=8,'dp'=4] {'dp'}, dimensions={0}, use_global_device_ids=true | all-gather | bytes 81920 | tf_op jit(solution)/shard_map/all_gather | solution.py:79
  129.7 4.2 %reshape_squeeze.7 = f32[16,512,64]{2,1,0:T(8,128)} reshape(f32[1,16,32768]{2,1,0:T(8,128)} %get-tuple-element.4) | data formatting | bytes 4194304 | tf_op jit(solution)/shard_map/reshape;squeeze | solution.py:63
  133.9 3.9 copy.19
  140.6 4.1 stack_reshape.6
  144.7 56.1 %all-reduce.5.cloned.1.call-done = f32[64,1024]{1,0:T(8,128)} async-done(((f32[64,1024]{1,0:T(8,128)}), f32[64,1024]{1,0:T(8,128)}) %all-reduce.5.cloned.1.call-update) | async-done | bytes 262160 | tf_op jit(solution)/shard_map/psum | solution.py:83
  201.9 5.7 %psum.29 = f32[64]{0:T(128)S(1)} all-reduce(f32[64]{0:T(128)S(1)} %multiply_reduce_fusion.1), channel_id=1, replica_groups=mesh['tp'=8,'dp'=4] {'dp'}, use_global_device_ids=true, to_apply=%region_11.12 | all-reduce | flops 64 | bytes 512 | tf_op jit(solution)/shard_map/psum | solution.py:84
  209.7 6.6 %all-reduce.1 = f32[64]{0:T(128)S(1)} all-reduce(f32[64]{0:T(128)S(1)} %get-tuple-element.2), channel_id=9, replica_groups=mesh['tp'=8,'dp'=4] {'dp'}, use_global_device_ids=true, to_apply=%region_14.15.clone | all-reduce | flops 64 | bytes 512
  223.7 5.1 %reduce-scatter.21.cloned.1.call-done = f32[16,256]{1,0:T(8,128)} async-done(((f32[64,256]{1,0:T(8,128)}), f32[16,256]{1,0:T(8,128)}) %reduce-scatter.21.cloned.1.call-update) | async-done | bytes 16400 | tf_op jit(solution)/shard_map/reduce_scatter | solution.py:51
  228.8 22.0 %reduce-scatter.23.cloned.1.call-done = f32[16,256]{1,0:T(8,128)} async-done(((f32[64,256]{1,0:T(8,128)}), f32[16,256]{1,0:T(8,128)}) %reduce-scatter.23.cloned.1.call-update) | async-done | bytes 16400 | tf_op jit(solution)/shard_map/reduce_scatter | solution.py:51
  250.8 22.0 %reduce-scatter.25.cloned.1.call-done = f32[16,256]{1,0:T(8,128)} async-done(((f32[64,256]{1,0:T(8,128)}), f32[16,256]{1,0:T(8,128)}) %reduce-scatter.25.cloned.1.call-update) | async-done | bytes 16400 | tf_op jit(solution)/shard_map/reduce_scatter | solution.py:51
  276.3 19.1 %reduce-scatter.27.cloned.1.call-done = f32[16,512]{1,0:T(8,128)} async-done(((f32[64,512]{1,0:T(8,128)}), f32[16,512]{1,0:T(8,128)}) %reduce-scatter.27.cloned.1.call-update) | async-done | bytes 32784 | tf_op jit(solution)/shard_map/reduce_scatter | solution.py:51
  302.3 15.1 %reduce-scatter.29.cloned.1.call-done = f32[16,512]{1,0:T(8,128)} async-done(((f32[64,512]{1,0:T(8,128)}), f32[16,512]{1,0:T(8,128)}) %reduce-scatter.29.cloned.1.call-update) | async-done | bytes 32784 | tf_op jit(solution)/shard_map/reduce_scatter | solution.py:51
  318.3 5.2 %all_gather.7 = bf16[64,512]{1,0:T(8,128)(2,1)S(1)} all-gather(bf16[16,512]{1,0:T(8,128)(2,1)S(1)} %fusion.58), channel_id=1, replica_groups=mesh['tp'=8,'dp'=4] {'dp'}, dimensions={0}, use_global_device_ids=true | all-gather | bytes 81920 | tf_op jit(solution)/shard_map/all_gather | solution.py:79
  325.8 4.0 stack_reshape.7
  329.9 3.9 pad_maximum_fusion
  333.7 63.3 %all-reduce.7.cloned.1.call-done = f32[64,1024]{1,0:T(8,128)} async-done(((f32[64,1024]{1,0:T(8,128)}), f32[64,1024]{1,0:T(8,128)}) %all-reduce.7.cloned.1.call-update) | async-done | bytes 262160 | tf_op jit(solution)/shard_map/psum | solution.py:83
  398.1 5.7 %psum.31 = f32[64]{0:T(128)S(1)} all-reduce(f32[64]{0:T(128)S(1)} %multiply_reduce_fusion), channel_id=1, replica_groups=mesh['tp'=8,'dp'=4] {'dp'}, use_global_device_ids=true, to_apply=%region_23.24 | all-reduce | flops 64 | bytes 512 | tf_op jit(solution)/shard_map/psum | solution.py:84
  (103 shorter events, 54.6 us)
Async XLA Ops:
  7.2 7.0 %copy-start.1 = (bf16[64,1024]{1,0:T(8,128)(2,1)S(1)}, bf16[64,1024]{1,0:T(8,128)(2,1)}, u32[]{:S(2)}) copy-start(bf16[64,1024]{1,0:T(8,128)(2,1)} %param.12) | copy-start | bytes 393220
  7.2 7.0 %copy-start.5 = (bf16[2,1024,512]{2,1,0:T(8,128)(2,1)S(1)}, bf16[2,1024,512]{2,1,0:T(8,128)(2,1)}, u32[]{:S(2)}) copy-start(bf16[2,1024,512]{2,1,0:T(8,128)(2,1)} %param.17) | copy-start | bytes 6291460
  7.2 30.9 %reduce-scatter.11.cloned.1.call-start = ((), (), s32[]{:S(2)}) async-start(), calls=%async_computation.10 | async-start | bytes 81920 | tf_op jit(solution)/shard_map/reduce_scatter | solution.py:51
  10.1 44.6 %reduce-scatter.13.cloned.1.call-start = ((), (), s32[]{:S(2)}) async-start(), calls=%async_computation.11 | async-start | bytes 81920 | tf_op jit(solution)/shard_map/reduce_scatter | solution.py:51
  12.1 64.6 %reduce-scatter.15.cloned.1.call-start = ((), (), s32[]{:S(2)}) async-start(), calls=%async_computation.12 | async-start | bytes 81920 | tf_op jit(solution)/shard_map/reduce_scatter | solution.py:51
  14.1 85.1 %reduce-scatter.17.cloned.1.call-start = ((), (), s32[]{:S(2)}) async-start(), calls=%async_computation.13 | async-start | bytes 163840 | tf_op jit(solution)/shard_map/reduce_scatter | solution.py:51
  15.2 106.0 %reduce-scatter.19.cloned.1.call-start = ((), (), s32[]{:S(2)}) async-start(), calls=%async_computation.14 | async-start | bytes 163840 | tf_op jit(solution)/shard_map/reduce_scatter | solution.py:51
  17.4 183.4 %all-reduce.5.cloned.1.call-start = ((), (), s32[]{:S(2)}) async-start(), calls=%async_computation.15 | async-start | bytes 524288 | tf_op jit(solution)/shard_map/psum | solution.py:83
  24.5 12.2 %copy-start.3 = (f32[2,256]{1,0:T(2,128)S(1)}, f32[2,256]{1,0:T(2,128)}, u32[]{:S(2)}) copy-start(f32[2,256]{1,0:T(2,128)} %param.20) | copy-start | bytes 6148
  24.5 12.2 %copy-start.4 = (f32[2,128]{1,0:T(2,128)S(1)}, f32[2,128]{1,0:T(2,128)}, u32[]{:S(2)}) copy-start(f32[2,128]{1,0:T(2,128)} %param.21) | copy-start | bytes 3076
  24.5 12.3 %copy-start.8 = (u32[32]{0:T(128)S(1)}, u32[32]{0:T(128)}, u32[]{:S(2)}) copy-start(u32[32]{0:T(128)} %constant.51) | copy-start | bytes 388
  129.6 99.2 %reduce-scatter.21.cloned.1.call-start = ((), (), s32[]{:S(2)}) async-start(), calls=%async_computation.16 | async-start | bytes 81920 | tf_op jit(solution)/shard_map/reduce_scatter | solution.py:51
  133.9 3.9 copy-start.2
  140.6 68.1 %copy-start.6 = (bf16[2,1024,256]{2,1,0:T(8,128)(2,1)S(1)}, bf16[2,1024,256]{2,1,0:T(8,128)(2,1)}, u32[]{:S(2)}) copy-start(bf16[2,1024,256]{2,1,0:T(8,128)(2,1)} %param.15) | copy-start | bytes 3145732
  140.6 75.7 %copy-start.7 = (bf16[2,1024,256]{2,1,0:T(8,128)(2,1)S(1)}, bf16[2,1024,256]{2,1,0:T(8,128)(2,1)}, u32[]{:S(2)}) copy-start(bf16[2,1024,256]{2,1,0:T(8,128)(2,1)} %param.19) | copy-start | bytes 3145732
  209.6 41.2 %reduce-scatter.23.cloned.1.call-start = ((), (), s32[]{:S(2)}) async-start(), calls=%async_computation.17 | async-start | bytes 81920 | tf_op jit(solution)/shard_map/reduce_scatter | solution.py:51
  217.1 55.7 %reduce-scatter.25.cloned.1.call-start = ((), (), s32[]{:S(2)}) async-start(), calls=%async_computation.18 | async-start | bytes 81920 | tf_op jit(solution)/shard_map/reduce_scatter | solution.py:51
  219.1 76.2 %reduce-scatter.27.cloned.1.call-start = ((), (), s32[]{:S(2)}) async-start(), calls=%async_computation.19 | async-start | bytes 163840 | tf_op jit(solution)/shard_map/reduce_scatter | solution.py:51
  221.3 96.1 %reduce-scatter.29.cloned.1.call-start = ((), (), s32[]{:S(2)}) async-start(), calls=%async_computation.20 | async-start | bytes 163840 | tf_op jit(solution)/shard_map/reduce_scatter | solution.py:51
  223.6 173.4 %all-reduce.7.cloned.1.call-start = ((), (), s32[]{:S(2)}) async-start(), calls=%async_computation.21 | async-start | bytes 524288 | tf_op jit(solution)/shard_map/psum | solution.py:83
  325.8 4.0 copy-start
Sparse Core Ops, SparseCore 0:
  10.4 22.2 reduce-scatter.10
  35.1 19.5 reduce-scatter.12
  57.1 19.5 reduce-scatter.14
  79.6 19.6 reduce-scatter.16
  101.5 19.6 reduce-scatter.18
  129.8 70.9 all-reduce.4
  209.7 19.0 reduce-scatter.20
  231.2 19.5 reduce-scatter.22
  253.2 19.5 reduce-scatter.24
  275.6 19.6 reduce-scatter.26
  297.8 19.6 reduce-scatter.28
  326.0 71.0 all-reduce.6
where the time goes:
time: 414 us; the launch traced here: 412 us
  waiting for transfers between devices  278 us (67%)
  blocking collectives  36.8 us (9%)
  local copies, waits for them, and re-layouts  34.7 us (8%)
  matrix products  32.5 us (8%)
  between operations  15.1 us (4%)
  other arithmetic  14.5 us (4%)
    reduce_scatter x10, waiting for transfers between devices, local(): lax.psum_scatter(partials + (squares_part,), 'dp', scatter_dimension=0, t...  159 us
    psum x2, waiting for transfers between devices, local(): out_rows = lax.psum(partial_out, 'tp')  119 us
    dot_general x10, matrix products, local(): jnp.dot(normed, weights[section_index], preferred_element_type=jnp.float32)  16.9 us
    unnamed x2, blocking collectives  15 us
    another operation x4, local copies, waits for them, and re-layouts, local(): recurrent_state[section_index].reshape(local_seqs, value_cols, KEY)  14.9 us
    psum x2, blocking collectives, local(): out_squares = lax.psum(jnp.sum(out_rows * out_rows, axis=1), 'dp')  11.3 us
    dot_general x6, matrix products, spread_heads(): return jnp.einsum('bhk,hc->bck', shaped, spread, precision=highest)  11.2 us
    all_gather x2, blocking collectives, local(): lax.all_gather(mixed, 'dp', axis=0, tiled=True)  10.5 us
  transfers between devices with their start and end apart: 12, of which 11 were waited for; matrix products, arithmetic and copies ran while one was open for 16% of the time, Pallas kernels for 0%

commit v1 on v0

--- a/solution.py
+++ b/solution.py
@@ -80,7 +80,11 @@
             out_weight,
             preferred_element_type=jnp.float32,
         )
-        out_rows = lax.psum(partial_out, "tp")
+        n_dev = lax.axis_size("tp")
+        out_rows, hop = (partial_out, 1)
+        while hop < n_dev:
+            out_rows = out_rows + lax.ppermute(out_rows, "tp", [(i, i ^ hop) for i in range(n_dev)])
+            hop = 2 * hop
         out_squares = lax.psum(jnp.sum(out_rows * out_rows, axis=1), "dp")
         residual = (
             wide_float

time: 414 us -> 337 us (0.81)
  waiting for transfers between devices: 278 us -> 192 us
  starting transfers between devices: 0.5 us -> 11.5 us
    psum x2 -> x0, waiting for transfers between devices: 119 us -> none  [local(): out_rows = lax.psum(partial_out, 'tp')]
    ppermute x0 -> x6, waiting for transfers between devices: none -> 30.9 us  [local(): lax.ppermute(out_rows, 'tp', [(i, i ^ hop) for i in range(n_dev)])]
    ppermute x0 -> x6, starting transfers between devices: none -> 11.1 us  [local(): lax.ppermute(out_rows, 'tp', [(i, i ^ hop) for i in range(n_dev)])]
  transfers between devices with their start and end apart: 12 -> 16, of which waited for: 11 -> 14; matrix products, arithmetic and copies ran while one was open for 16% -> 20% of each run, Pallas kernels for 0% -> 0%
where the time goes in v1:
time: 337 us; the launch traced here: 336 us
  waiting for transfers between devices  192 us (57%)
  blocking collectives  36.6 us (11%)
  local copies, waits for them, and re-layouts  35.9 us (11%)
  matrix products  33.2 us (10%)
  between operations  15.1 us (4%)
  starting transfers between devices  11.5 us (3%)
  other arithmetic  10.8 us (3%)
    reduce_scatter x10, waiting for transfers between devices, local(): lax.psum_scatter(partials + (squares_part,), 'dp', scatter_dimension=0, t...  161 us
    ppermute x6, waiting for transfers between devices, local(): lax.ppermute(out_rows, 'tp', [(i, i ^ hop) for i in range(n_dev)])  30.9 us
    dot_general x10, matrix products, local(): jnp.dot(normed, weights[section_index], preferred_element_type=jnp.float32)  18.9 us
    another operation x4, local copies, waits for them, and re-layouts, local(): recurrent_state[section_index].reshape(local_seqs, value_cols, KEY)  14.9 us
    unnamed x2, blocking collectives  14.3 us
    psum x2, blocking collectives, local(): out_squares = lax.psum(jnp.sum(out_rows * out_rows, axis=1), 'dp')  11.6 us
    dot_general x6, matrix products, spread_heads(): return jnp.einsum('bhk,hc->bck', shaped, spread, precision=highest)  11.2 us
    ppermute x6, starting transfers between devices, local(): lax.ppermute(out_rows, 'tp', [(i, i ^ hop) for i in range(n_dev)])  11.1 us
  transfers between devices with their start and end apart: 16, of which 14 were waited for; matrix products, arithmetic and copies ran while one was open for 20% of the time, Pallas kernels for 0%

profile of v1, /device:TPU:0, one launch (start us, length us, event | category | flops | bytes accessed | tf_op | source)
XLA Modules:
  0.0 335.5 jit_solution(8048111818992998427)
XLA Ops:
  17.6 3.9 %fusion.83 = (f32[1,16,32768]{2,1,0:T(8,128)}, f32[1,16,32768]{2,1,0:T(8,128)S(1)}) fusion(f32[2,16,32768]{2,1,0:T(8,128)} %param.13), kind=kLoop, calls=%fused_computation.108 | loop fusion | bytes 8388608 | tf_op jit(solution)/shard_map/slice | solution.py:63
  28.3 8.4 %all-reduce = f32[64]{0:T(128)S(1)} all-reduce(f32[64]{0:T(128)S(1)} %fusion.41), channel_id=3, replica_groups=mesh['tp'=8,'dp'=4] {'dp'}, use_global_device_ids=true, to_apply=%region_2.3.clone | all-reduce | flops 64 | bytes 512
  38.1 16.7 %reduce-scatter.13.cloned.1.call-done = f32[16,256]{1,0:T(8,128)} async-done(((f32[64,256]{1,0:T(8,128)}), f32[16,256]{1,0:T(8,128)}) %reduce-scatter.13.cloned.1.call-update) | async-done | bytes 16400 | tf_op jit(solution)/shard_map/reduce_scatter | solution.py:51
  54.7 22.0 %reduce-scatter.15.cloned.1.call-done = f32[16,256]{1,0:T(8,128)} async-done(((f32[64,256]{1,0:T(8,128)}), f32[16,256]{1,0:T(8,128)}) %reduce-scatter.15.cloned.1.call-update) | async-done | bytes 16400 | tf_op jit(solution)/shard_map/reduce_scatter | solution.py:51
  80.2 19.1 %reduce-scatter.17.cloned.1.call-done = f32[16,512]{1,0:T(8,128)} async-done(((f32[64,512]{1,0:T(8,128)}), f32[16,512]{1,0:T(8,128)}) %reduce-scatter.17.cloned.1.call-update) | async-done | bytes 32784 | tf_op jit(solution)/shard_map/reduce_scatter | solution.py:51
  103.5 17.7 %reduce-scatter.19.cloned.1.call-done = f32[16,512]{1,0:T(8,128)} async-done(((f32[64,512]{1,0:T(8,128)}), f32[16,512]{1,0:T(8,128)}) %reduce-scatter.19.cloned.1.call-update) | async-done | bytes 32784 | tf_op jit(solution)/shard_map/reduce_scatter | solution.py:51
  122.1 5.2 %all_gather.6 = bf16[64,512]{1,0:T(8,128)(2,1)S(1)} all-gather(bf16[16,512]{1,0:T(8,128)(2,1)S(1)} %fusion.61), channel_id=1, replica_groups=mesh['tp'=8,'dp'=4] {'dp'}, dimensions={0}, use_global_device_ids=true | all-gather | bytes 81920 | tf_op jit(solution)/shard_map/all_gather | solution.py:79
  130.4 7.1 %collective-permute-done = f32[64,1024]{1,0:T(8,128)S(1)} collective-permute-done((f32[64,1024]{1,0:T(8,128)S(1)}, f32[64,1024]{1,0:T(8,128)S(1)}, u32[]{:S(2)}, u32[]{:S(2)}) %collective-permute-start) | collective-permute-done | bytes 262176 | tf_op jit(solution)/shard_map/ppermute | solution.py:86
  139.1 6.2 %collective-permute-done.1 = f32[64,1024]{1,0:T(8,128)S(1)} collective-permute-done((f32[64,1024]{1,0:T(8,128)S(1)}, f32[64,1024]{1,0:T(8,128)S(1)}, u32[]{:S(2)}, u32[]{:S(2)}) %collective-permute-start.1) | collective-permute-done | bytes 262176 | tf_op jit(solution)/shard_map/ppermute | solution.py:86
  147.8 4.2 %reshape_squeeze.7 = f32[16,512,64]{2,1,0:T(8,128)} reshape(f32[1,16,32768]{2,1,0:T(8,128)} %get-tuple-element.8) | data formatting | bytes 4194304 | tf_op jit(solution)/shard_map/reshape;squeeze | solution.py:63
  158.9 5.9 %psum.14 = f32[64]{0:T(128)S(1)} all-reduce(f32[64]{0:T(128)S(1)} %get-tuple-element.6), channel_id=1, replica_groups=mesh['tp'=8,'dp'=4] {'dp'}, use_global_device_ids=true, to_apply=%region_10.11 | all-reduce | flops 64 | bytes 512 | tf_op jit(solution)/shard_map/psum | solution.py:88
  167.0 5.9 %all-reduce.1 = f32[64]{0:T(128)S(1)} all-reduce(f32[64]{0:T(128)S(1)} %get-tuple-element.4), channel_id=9, replica_groups=mesh['tp'=8,'dp'=4] {'dp'}, use_global_device_ids=true, to_apply=%region_13.14.clone | all-reduce | flops 64 | bytes 512
  181.3 6.3 %reduce-scatter.21.cloned.1.call-done = f32[16,256]{1,0:T(8,128)} async-done(((f32[64,256]{1,0:T(8,128)}), f32[16,256]{1,0:T(8,128)}) %reduce-scatter.21.cloned.1.call-update) | async-done | bytes 16400 | tf_op jit(solution)/shard_map/reduce_scatter | solution.py:51
  187.5 22.0 %reduce-scatter.23.cloned.1.call-done = f32[16,256]{1,0:T(8,128)} async-done(((f32[64,256]{1,0:T(8,128)}), f32[16,256]{1,0:T(8,128)}) %reduce-scatter.23.cloned.1.call-update) | async-done | bytes 16400 | tf_op jit(solution)/shard_map/reduce_scatter | solution.py:51
  209.6 22.0 %reduce-scatter.25.cloned.1.call-done = f32[16,256]{1,0:T(8,128)} async-done(((f32[64,256]{1,0:T(8,128)}), f32[16,256]{1,0:T(8,128)}) %reduce-scatter.25.cloned.1.call-update) | async-done | bytes 16400 | tf_op jit(solution)/shard_map/reduce_scatter | solution.py:51
  235.1 19.3 %reduce-scatter.27.cloned.1.call-done = f32[16,512]{1,0:T(8,128)} async-done(((f32[64,512]{1,0:T(8,128)}), f32[16,512]{1,0:T(8,128)}) %reduce-scatter.27.cloned.1.call-update) | async-done | bytes 32784 | tf_op jit(solution)/shard_map/reduce_scatter | solution.py:51
  259.9 16.4 %reduce-scatter.29.cloned.1.call-done = f32[16,512]{1,0:T(8,128)} async-done(((f32[64,512]{1,0:T(8,128)}), f32[16,512]{1,0:T(8,128)}) %reduce-scatter.29.cloned.1.call-update) | async-done | bytes 32784 | tf_op jit(solution)/shard_map/reduce_scatter | solution.py:51
  277.2 5.4 %all_gather.7 = bf16[64,512]{1,0:T(8,128)(2,1)S(1)} all-gather(bf16[16,512]{1,0:T(8,128)(2,1)S(1)} %fusion.58), channel_id=1, replica_groups=mesh['tp'=8,'dp'=4] {'dp'}, dimensions={0}, use_global_device_ids=true | all-gather | bytes 81920 | tf_op jit(solution)/shard_map/all_gather | solution.py:79
  285.7 7.1 %collective-permute-done.3 = f32[64,1024]{1,0:T(8,128)S(1)} collective-permute-done((f32[64,1024]{1,0:T(8,128)S(1)}, f32[64,1024]{1,0:T(8,128)S(1)}, u32[]{:S(2)}, u32[]{:S(2)}) %collective-permute-start.3) | collective-permute-done | bytes 262176 | tf_op jit(solution)/shard_map/ppermute | solution.py:86
  297.1 4.0 %stack_reshape.6 = f32[1,16,32768]{2,1,0:T(8,128)} reshape(f32[16,512,64]{2,1,0:T(8,128)} %copy.20) | data formatting | bytes 4194304 | tf_op jit(solution)/shard_map/stack;reshape | solution.py:94
  303.9 4.1 %stack_reshape.7 = f32[1,16,32768]{2,1,0:T(8,128)} reshape(f32[16,512,64]{2,1,0:T(8,128)} %copy.21) | data formatting | bytes 4194304 | tf_op jit(solution)/shard_map/stack;reshape | solution.py:94
  310.5 3.9 %pad_maximum_fusion = f32[2,16,32768]{2,1,0:T(8,128)} fusion(f32[1,16,32768]{2,1,0:T(8,128)} %stack_reshape.7, f32[1,16,32768]{2,1,0:T(8,128)S(1)} %copy-done.2), kind=kLoop, calls=%fused_computation | loop fusion | flops 1048576 | bytes 8388608 | tf_op jit(solution)/shard_map/stack | solution.py:94
  314.4 7.6 %collective-permute-done.5 = f32[64,1024]{1,0:T(8,128)S(1)} collective-permute-done((f32[64,1024]{1,0:T(8,128)S(1)}, f32[64,1024]{1,0:T(8,128)S(1)}, u32[]{:S(2)}, u32[]{:S(2)}) %collective-permute-start.5) | collective-permute-done | bytes 262176 | tf_op jit(solution)/shard_map/ppermute | solution.py:86
  322.1 5.8 %psum.15 = f32[64]{0:T(128)S(1)} all-reduce(f32[64]{0:T(128)S(1)} %get-tuple-element.2), channel_id=1, replica_groups=mesh['tp'=8,'dp'=4] {'dp'}, use_global_device_ids=true, to_apply=%region_21.22 | all-reduce | flops 64 | bytes 512 | tf_op jit(solution)/shard_map/psum | solution.py:88
  (113 shorter events, 74.5 us)
Async XLA Ops:
  7.2 7.0 %copy-start.3 = (bf16[64,1024]{1,0:T(8,128)(2,1)S(1)}, bf16[64,1024]{1,0:T(8,128)(2,1)}, u32[]{:S(2)}) copy-start(bf16[64,1024]{1,0:T(8,128)(2,1)} %param.12) | copy-start | bytes 393220
  7.2 7.0 %copy-start.7 = (bf16[2,1024,512]{2,1,0:T(8,128)(2,1)S(1)}, bf16[2,1024,512]{2,1,0:T(8,128)(2,1)}, u32[]{:S(2)}) copy-start(bf16[2,1024,512]{2,1,0:T(8,128)(2,1)} %param.17) | copy-start | bytes 6291460
  7.2 30.9 %reduce-scatter.11.cloned.1.call-start = ((), (), s32[]{:S(2)}) async-start(), calls=%async_computation.10 | async-start | bytes 81920 | tf_op jit(solution)/shard_map/reduce_scatter | solution.py:51
  10.1 44.6 %reduce-scatter.13.cloned.1.call-start = ((), (), s32[]{:S(2)}) async-start(), calls=%async_computation.11 | async-start | bytes 81920 | tf_op jit(solution)/shard_map/reduce_scatter | solution.py:51
  12.1 64.6 %reduce-scatter.15.cloned.1.call-start = ((), (), s32[]{:S(2)}) async-start(), calls=%async_computation.12 | async-start | bytes 81920 | tf_op jit(solution)/shard_map/reduce_scatter | solution.py:51
  14.1 85.1 %reduce-scatter.17.cloned.1.call-start = ((), (), s32[]{:S(2)}) async-start(), calls=%async_computation.13 | async-start | bytes 163840 | tf_op jit(solution)/shard_map/reduce_scatter | solution.py:51
  15.2 106.0 %reduce-scatter.19.cloned.1.call-start = ((), (), s32[]{:S(2)}) async-start(), calls=%async_computation.14 | async-start | bytes 163840 | tf_op jit(solution)/shard_map/reduce_scatter | solution.py:51
  17.4 170.1 %reduce-scatter.21.cloned.1.call-start = ((), (), s32[]{:S(2)}) async-start(), calls=%async_computation.15 | async-start | bytes 81920 | tf_op jit(solution)/shard_map/reduce_scatter | solution.py:51
  24.5 12.2 %copy-start.5 = (f32[2,256]{1,0:T(2,128)S(1)}, f32[2,256]{1,0:T(2,128)}, u32[]{:S(2)}) copy-start(f32[2,256]{1,0:T(2,128)} %param.20) | copy-start | bytes 6148
  24.5 12.2 %copy-start.6 = (f32[2,128]{1,0:T(2,128)S(1)}, f32[2,128]{1,0:T(2,128)}, u32[]{:S(2)}) copy-start(f32[2,128]{1,0:T(2,128)} %param.21) | copy-start | bytes 3076
  24.5 12.3 %copy-start.8 = (u32[32]{0:T(128)S(1)}, u32[32]{0:T(128)}, u32[]{:S(2)}) copy-start(u32[32]{0:T(128)} %constant.51) | copy-start | bytes 388
  128.9 8.6 %collective-permute-start = (f32[64,1024]{1,0:T(8,128)S(1)}, f32[64,1024]{1,0:T(8,128)S(1)}, u32[]{:S(2)}, u32[]{:S(2)}) collective-permute-start(f32[64,1024]{1,0:T(8,128)S(1)} %fusion.10), channel_id=1, source_target_pairs={{0,4},{4,0},{8,12},{12,8},{16,20},{20,16},{24,28},{28,24},{1,5},{5... | collective-permute-start | bytes 786440 | tf_op jit(solution)/shard_map/ppermute | solution.py:86
  137.5 7.8 %collective-permute-start.1 = (f32[64,1024]{1,0:T(8,128)S(1)}, f32[64,1024]{1,0:T(8,128)S(1)}, u32[]{:S(2)}, u32[]{:S(2)}) collective-permute-start(f32[64,1024]{1,0:T(8,128)S(1)} %add.135), channel_id=1, source_target_pairs={{0,8},{4,12},{8,0},{12,4},{16,24},{20,28},{24,16},{28,20},{1,9},{5... | collective-permute-start | bytes 786440 | tf_op jit(solution)/shard_map/ppermute | solution.py:86
  145.4 13.4 %collective-permute-start.2 = (f32[64,1024]{1,0:T(8,128)S(1)}, f32[64,1024]{1,0:T(8,128)S(1)}, u32[]{:S(2)}, u32[]{:S(2)}) collective-permute-start(f32[64,1024]{1,0:T(8,128)S(1)} %add.136), channel_id=1, source_target_pairs={{0,16},{4,20},{8,24},{12,28},{16,0},{20,4},{24,8},{28,12},{1,17},{... | collective-permute-start | bytes 786440 | tf_op jit(solution)/shard_map/ppermute | solution.py:86
  152.0 3.9 %copy-start.4 = (f32[2,1024]{1,0:T(2,128)S(1)}, f32[2,1024]{1,0:T(2,128)}, u32[]{:S(2)}) copy-start(f32[2,1024]{1,0:T(2,128)} %param.23) | copy-start | bytes 24580
  166.9 42.6 %reduce-scatter.23.cloned.1.call-start = ((), (), s32[]{:S(2)}) async-start(), calls=%async_computation.16 | async-start | bytes 81920 | tf_op jit(solution)/shard_map/reduce_scatter | solution.py:51
  174.8 56.8 %reduce-scatter.25.cloned.1.call-start = ((), (), s32[]{:S(2)}) async-start(), calls=%async_computation.17 | async-start | bytes 81920 | tf_op jit(solution)/shard_map/reduce_scatter | solution.py:51
  176.7 77.6 %reduce-scatter.27.cloned.1.call-start = ((), (), s32[]{:S(2)}) async-start(), calls=%async_computation.18 | async-start | bytes 163840 | tf_op jit(solution)/shard_map/reduce_scatter | solution.py:51
  179.0 97.3 %reduce-scatter.29.cloned.1.call-start = ((), (), s32[]{:S(2)}) async-start(), calls=%async_computation.19 | async-start | bytes 163840 | tf_op jit(solution)/shard_map/reduce_scatter | solution.py:51
  284.1 8.6 %collective-permute-start.3 = (f32[64,1024]{1,0:T(8,128)S(1)}, f32[64,1024]{1,0:T(8,128)S(1)}, u32[]{:S(2)}, u32[]{:S(2)}) collective-permute-start(f32[64,1024]{1,0:T(8,128)S(1)} %fusion.4), channel_id=1, source_target_pairs={{0,4},{4,0},{8,12},{12,8},{16,20},{20,16},{24,28},{28,24},{1,5},{5... | collective-permute-start | bytes 786440 | tf_op jit(solution)/shard_map/ppermute | solution.py:86
  292.8 15.2 %collective-permute-start.4 = (f32[64,1024]{1,0:T(8,128)S(1)}, f32[64,1024]{1,0:T(8,128)S(1)}, u32[]{:S(2)}, u32[]{:S(2)}) collective-permute-start(f32[64,1024]{1,0:T(8,128)S(1)} %add.148), channel_id=1, source_target_pairs={{0,8},{4,12},{8,0},{12,4},{16,24},{20,28},{24,16},{28,20},{1,9},{5... | collective-permute-start | bytes 786440 | tf_op jit(solution)/shard_map/ppermute | solution.py:86
  297.1 4.0 %copy-start.1 = (f32[16,512,64]{1,2,0:T(8,128)S(1)}, f32[16,512,64]{1,2,0:T(8,128)}, u32[]{:S(2)}) copy-start(f32[16,512,64]{1,2,0:T(8,128)} %copy-done) | copy-start | bytes 6291460
  303.9 6.6 %copy-start.2 = (f32[1,16,32768]{2,1,0:T(8,128)S(1)}, f32[1,16,32768]{2,1,0:T(8,128)}, u32[]{:S(2)}) copy-start(f32[1,16,32768]{2,1,0:T(8,128)} %stack_reshape.6) | copy-start | bytes 6291460
  308.0 14.0 %collective-permute-start.5 = (f32[64,1024]{1,0:T(8,128)S(1)}, f32[64,1024]{1,0:T(8,128)S(1)}, u32[]{:S(2)}, u32[]{:S(2)}) collective-permute-start(f32[64,1024]{1,0:T(8,128)S(1)} %add.149), channel_id=1, source_target_pairs={{0,16},{4,20},{8,24},{12,28},{16,0},{20,4},{24,8},{28,12},{1,17},{... | collective-permute-start | bytes 786440 | tf_op jit(solution)/shard_map/ppermute | solution.py:86
  (1 other events, 1.4 us)
Sparse Core Ops, SparseCore 0:
  10.4 22.2 reduce-scatter.10
  35.1 19.5 reduce-scatter.12
  57.1 19.5 reduce-scatter.14
  79.6 19.6 reduce-scatter.16
  101.5 19.6 reduce-scatter.18
  167.1 20.4 reduce-scatter.20
  190.0 19.5 reduce-scatter.22
  212.0 19.5 reduce-scatter.24
  234.6 19.6 reduce-scatter.26
  256.6 19.6 reduce-scatter.28
